TPU v7x, 32 devices: a whole 2x2x4 slice. The times are simulated.
32 devices in a mesh: grp: 2 (over y), sp: 4 (over z), tp: 4 (over x, core).
Axes of the slice: x: 2, y: 2, z: 4, core: 2. Of those that a mesh axis runs over, the one named last changes fastest.
Arguments:
- stream: bfloat16 [6144, 4096], P(('grp', 'sp'), 'tp'), parts along dimension 0, may hold values from -400 to 400
- in_weight: bfloat16 [2, 1024, 4096], P(None, 'sp', 'tp'), may hold values from -0.09375 to 0.09375
- out_weight: bfloat16 [2, 1024, 4096], P(None, 'sp', 'tp'), may hold values from -0.1875 to 0.1875
- group_mix: bfloat16 [2, 4, 256, 256], replicated, may hold values from -0.375 to 0.375
- pool_gain: float32 [2, 1024], replicated, may hold values from 0.1 to 1.9
- norm_gain: float32 [2, 4096], P(None, 'tp'), may hold values from 0.1 to 1.9
- norm_shift: float32 [2, 4096], P(None, 'tp'), may hold values from -3 to 3
Outputs:
- refined: bfloat16 [6144, 4096], P(('grp', 'sp'), 'tp'), parts along dimension 0
There are 2 independent parts, one for each index of `grp`. A program takes and returns all parts, laid end to end along the dimension named above; an argument that names none is the same for every part. Nothing has to cross between parts.
All inputs are finite; a program needn't handle non-finite values.
Results may differ from a plain program's by a relative error of at most 0.015.
Values may be sent and summed in bfloat16 or wider, within the bound.
A program may use at most 64 MiB of HBM per device.

v0:
```python
import jax
import jax.numpy as jnp
from jax import lax
from jax.sharding import PartitionSpec as P

D = 4096
POOL = 1024
GROUPS = 4
GROUP_WIDTH = 256
LAYERS = 2
epsilon = 1e-05


def passed_along(block, axis, distance):
    devices = range(lax.axis_size(axis))
    route = [(i - distance, i) for i in devices if i - distance in devices]
    return lax.ppermute(block, axis, route)


def pooled_windows(hidden, tok_start):
    reach = 2**GROUPS - 1
    length = hidden.shape[1]
    channels = hidden.shape[0]
    earlier = passed_along(hidden[:, length - reach :], "sp", 1)
    extended = jnp.concatenate([earlier, hidden], axis=1).astype(jnp.float32)
    group_ids = (jnp.arange(channels, dtype=jnp.int32) // GROUP_WIDTH)[:, None]
    running = extended
    window_sums = jnp.zeros((channels, length), jnp.float32)
    for octave in range(GROUPS):
        offset = 2**octave
        running = running[:, offset:] + running[:, : running.shape[1] - offset]
        window_sums = jnp.where(
            group_ids == octave, running[:, running.shape[1] - length :], window_sums
        )
    positions = (tok_start + jnp.arange(length, dtype=jnp.int32) + 1).astype(jnp.float32)
    widths = jnp.exp2((group_ids + 1).astype(jnp.float32))
    counts = jnp.minimum(positions[None, :], widths)
    return (window_sums / counts - hidden.astype(jnp.float32)).astype(jnp.bfloat16)


def per_device(stream, in_weight, out_weight, group_mix, pool_gain, norm_gain, norm_shift):
    tok_rows = stream.shape[0]
    tok_start = lax.axis_index("sp") * tok_rows
    alpha = (2.0 * LAYERS) ** 0.25
    contract_rows = (((0,), (0,)), ((), ()))
    contract_cols = (((1,), (1,)), ((), ()))
    current = stream
    for layer_index in range(LAYERS):
        whole_in = lax.all_gather(in_weight[layer_index], "sp", axis=0, tiled=True)
        partial_value = lax.dot_general(
            whole_in, current, contract_cols, preferred_element_type=jnp.float32
        )
        hidden = lax.psum(partial_value.astype(jnp.bfloat16), "tp")
        pooled = pooled_windows(hidden, tok_start)
        grouped = pooled.reshape(GROUPS, GROUP_WIDTH, tok_rows)
        mixed = jnp.einsum(
            "gio,git->got", group_mix[layer_index], grouped, preferred_element_type=jnp.float32
        )
        gains = pool_gain[layer_index].reshape(GROUPS, GROUP_WIDTH, 1)
        scaled = (mixed * gains).astype(jnp.bfloat16).reshape(POOL, tok_rows)
        branch = lax.dot_general(
            scaled,
            lax.all_gather(out_weight[layer_index], "sp", axis=0, tiled=True),
            contract_rows,
            preferred_element_type=jnp.float32,
        )
        summed = alpha * current.astype(jnp.float32) + branch
        row_sum, row_squares = lax.psum(
            (jnp.sum(summed, axis=1), jnp.sum(summed * summed, axis=1)), "tp"
        )
        row_mean = row_sum / D
        row_var = row_squares / D - row_mean * row_mean
        normed = (summed - row_mean[:, None]) * lax.rsqrt(row_var + epsilon)[:, None]
        current = (
            normed * norm_gain[layer_index][None, :] + norm_shift[layer_index][None, :]
        ).astype(jnp.bfloat16)
    return current


def solution(mesh):
    in_specs = (
        P(("grp", "sp"), "tp"),
        P(None, "sp", "tp"),
        P(None, "sp", "tp"),
        P(),
        P(),
        P(None, "tp"),
        P(None, "tp"),
    )
    out_specs = P(("grp", "sp"), "tp")
    return jax.shard_map(
        per_device, mesh=mesh, in_specs=in_specs, out_specs=out_specs, check_vma=False
    )
```

profile of v0, /device:TPU:0, one launch (start us, length us, event | category | flops | bytes accessed | tf_op | source)
XLA Modules:
  0.0 312.8 jit_solution(13905823871252964514)
XLA Ops:
  6.5 2.2 fusion.49
  8.9 48.5 %all-gather.9.cloned.1.call-done = bf16[1,1024,1024]{2,1,0:T(8,128)(2,1)} async-done(((bf16[1,256,1024]{2,1,0:T(8,128)(2,1)}), bf16[1,1024,1024]{2,1,0:T(8,128)(2,1)}) %all-gather.9.cloned.1.call-update) | async-done | bytes 2097168 | tf_op jit(solution)/shard_map/all_gather | solution.py:49
  57.3 5.0 %fusion.22 = bf16[1024,768]{1,0:T(8,128)(2,1)} fusion(bf16[768,1024]{1,0:T(8,128)(2,1)} %param.7, bf16[1,1024,1024]{2,1,0:T(8,128)(2,1)} %all-gather.9.cloned.1.call-done), kind=kOutput, calls=%fused_computation.40 | convolution fusion | flops 1611399168 | bytes 5242880 | tf_op jit(solution)/shard_map/dot_general | solution.py:50
  62.4 1.1 fusion.48
  64.3 39.9 %all-reduce.5.cloned.1.call-done = bf16[1024,768]{1,0:T(8,128)(2,1)} async-done(((bf16[1024,768]{1,0:T(8,128)(2,1)}), bf16[1024,768]{1,0:T(8,128)(2,1)}) %all-reduce.5.cloned.1.call-update) | async-done | bytes 1572880 | tf_op jit(solution)/shard_map/psum | solution.py:53
  105.3 3.4 %collective-permute-start = (bf16[1024,15]{1,0:T(8,128)(2,1)S(1)}, bf16[1024,15]{1,0:T(8,128)(2,1)S(1)}, u32[]{:S(2)}, u32[]{:S(2)}) collective-permute-start(bf16[1024,15]{1,0:T(8,128)(2,1)S(1)} %slice.138), channel_id=1, source_target_pairs={{0,4},{4,8},{8,12},{1,5},{5,9},{9,13},{2,6},{6,10},{10,14},{3,7},{... | collective-permute-start | bytes 92168 | tf_op jit(solution)/shard_map/ppermute | solution.py:17
  108.7 5.4 %collective-permute-done = bf16[1024,15]{1,0:T(8,128)(2,1)S(1)} collective-permute-done((bf16[1024,15]{1,0:T(8,128)(2,1)S(1)}, bf16[1024,15]{1,0:T(8,128)(2,1)S(1)}, u32[]{:S(2)}, u32[]{:S(2)}) %collective-permute-start) | collective-permute-done | bytes 30752 | tf_op jit(solution)/shard_map/ppermute | solution.py:17
  114.1 2.3 maximum_convert_fusion
  119.9 4.1 %fusion.1 = bf16[1024,768]{1,0:T(8,128)(2,1)S(1)} fusion(f32[1024,782]{1,0:T(8,128)S(1)} %slice_add_fusion.5, f32[1024,780]{1,0:T(8,128)S(1)} %slice_add_fusion.4, f32[1024,776]{1,0:T(8,128)S(1)} %slice_add_fusion.3, bf16[1024,768]{1,0:T(8,128)(2,1)S(1)} %copy-done, f32[1024]{0:T(1024)S(1)} %fusion.44, f32[768]{0:T(1024)S(1)} %add_convert_fusion.2, ...), kind=kLoop, calls=%fused_computation.9 | loop fusion | flops 7864320 | bytes 15739904 | tf_op jit(solution)/shard_map/convert_element_type | solution.py:38
  124.7 26.8 %all-gather.11.cloned.1.call-done = bf16[1,1024,1024]{2,1,0:T(8,128)(2,1)} async-done(((bf16[1,256,1024]{2,1,0:T(8,128)(2,1)}), bf16[1,1024,1024]{2,1,0:T(8,128)(2,1)}) %all-gather.11.cloned.1.call-update) | async-done | bytes 2097168 | tf_op jit(solution)/shard_map/all_gather | solution.py:63
  151.5 5.8 %fusion.47 = (f32[768]{0:T(1024)S(1)}, f32[768]{0:T(1024)S(1)}, f32[768,1024]{1,0:T(8,128)}) fusion(bf16[1024,768]{1,0:T(8,128)(2,1)S(1)} %bitcast.56, bf16[1,1024,1024]{2,1,0:T(8,128)(2,1)} %all-gather.11.cloned.1.call-done, bf16[768,1024]{1,0:T(8,128)(2,1)} %param.7), kind=kOutput, calls=%fused_computation.70 | convolution fusion | flops 1615329792 | bytes 8394752 | tf_op jit(solution)/shard_map/dot_general | solution.py:61
  157.3 6.5 %all-reduce.1 = (f32[768]{0:T(1024)S(1)}, f32[768]{0:T(1024)S(1)}) all-reduce(f32[768]{0:T(1024)S(1)} %get-tuple-element.8, f32[768]{0:T(1024)S(1)} %get-tuple-element.7), channel_id=1, replica_groups=mesh['grp'=2,'sp'=4,'tp'=4] {'tp'}, use_global_device_ids=true, to_apply=%region_4.5 | all-reduce | flops 1536 | bytes 12288 | tf_op jit(solution)/shard_map/psum | solution.py:68
  163.8 33.6 %all-gather.13.cloned.1.call-done = bf16[1,1024,1024]{2,1,0:T(8,128)(2,1)} async-done(((bf16[1,256,1024]{2,1,0:T(8,128)(2,1)}), bf16[1,1024,1024]{2,1,0:T(8,128)(2,1)}) %all-gather.13.cloned.1.call-update) | async-done | bytes 2097168 | tf_op jit(solution)/shard_map/all_gather | solution.py:49
  197.4 5.6 %fusion.28 = bf16[1024,768]{1,0:T(8,128)(2,1)} fusion(bf16[1,1024,1024]{2,1,0:T(8,128)(2,1)} %all-gather.13.cloned.1.call-done, f32[768,1024]{1,0:T(8,128)} %get-tuple-element.27, f32[1024]{0:T(1024)S(1)} %bitcast.61, f32[1024]{0:T(1024)S(1)} %bitcast.59, f32[768]{0:T(1024)S(1)} %get-tuple-element.26, f32[768]{0:T(1024)S(1)} %get-tuple-element.25), kind=kOutput, calls=%fused_computation.42 | convolution fusion | flops 1615331328 | bytes 6830080 | tf_op jit(solution)/shard_map/dot_general | solution.py:50
  203.7 41.2 %all-reduce.7.cloned.1.call-done = bf16[1024,768]{1,0:T(8,128)(2,1)} async-done(((bf16[1024,768]{1,0:T(8,128)(2,1)}), bf16[1024,768]{1,0:T(8,128)(2,1)}) %all-reduce.7.cloned.1.call-update) | async-done | bytes 1572880 | tf_op jit(solution)/shard_map/psum | solution.py:53
  246.0 3.6 %collective-permute-start.1 = (bf16[1024,15]{1,0:T(8,128)(2,1)S(1)}, bf16[1024,15]{1,0:T(8,128)(2,1)S(1)}, u32[]{:S(2)}, u32[]{:S(2)}) collective-permute-start(bf16[1024,15]{1,0:T(8,128)(2,1)S(1)} %slice.149), channel_id=1, source_target_pairs={{0,4},{4,8},{8,12},{1,5},{5,9},{9,13},{2,6},{6,10},{10,14},{3,7},{... | collective-permute-start | bytes 92168 | tf_op jit(solution)/shard_map/ppermute | solution.py:17
  249.6 5.5 %collective-permute-done.1 = bf16[1024,15]{1,0:T(8,128)(2,1)S(1)} collective-permute-done((bf16[1024,15]{1,0:T(8,128)(2,1)S(1)}, bf16[1024,15]{1,0:T(8,128)(2,1)S(1)}, u32[]{:S(2)}, u32[]{:S(2)}) %collective-permute-start.1) | collective-permute-done | bytes 30752 | tf_op jit(solution)/shard_map/ppermute | solution.py:17
  255.2 2.2 maximum_convert_fusion.1
  260.9 4.1 %fusion.3 = bf16[1024,768]{1,0:T(8,128)(2,1)S(1)} fusion(f32[1024,782]{1,0:T(8,128)S(1)} %slice_add_fusion.2, f32[1024,780]{1,0:T(8,128)S(1)} %slice_add_fusion.1, f32[1024,776]{1,0:T(8,128)S(1)} %slice_add_fusion, bf16[1024,768]{1,0:T(8,128)(2,1)S(1)} %copy-done.1, f32[1024]{0:T(1024)S(1)} %fusion.44, f32[768]{0:T(1024)S(1)} %add_convert_fusion.2, ...), kind=kLoop, calls=%fused_computation.11 | loop fusion | flops 7864320 | bytes 15739904 | tf_op jit(solution)/shard_map/convert_element_type | solution.py:38
  265.0 1.8 multiply_convert_fusion
  266.8 25.3 %all-gather.15.cloned.1.call-done = bf16[1,1024,1024]{2,1,0:T(8,128)(2,1)} async-done(((bf16[1,256,1024]{2,1,0:T(8,128)(2,1)}), bf16[1,1024,1024]{2,1,0:T(8,128)(2,1)}) %all-gather.15.cloned.1.call-update) | async-done | bytes 2097168 | tf_op jit(solution)/shard_map/all_gather | solution.py:63
  292.1 5.6 %fusion.46 = (f32[768]{0:T(1024)S(1)}, f32[768]{0:T(1024)S(1)}, f32[768,1024]{1,0:T(8,128)S(1)}) fusion(bf16[1024,768]{1,0:T(8,128)(2,1)} %bitcast.55, bf16[1,1024,1024]{2,1,0:T(8,128)(2,1)} %all-gather.15.cloned.1.call-done, f32[1024]{0:T(1024)S(1)} %bitcast.62, f32[1024]{0:T(1024)S(1)} %bitcast.60, f32[768]{0:T(1024)S(1)} %get-tuple-element.26, ...), kind=kOutput, calls=%fused_computation.69 | convolution fusion | flops 1619261952 | bytes 9981952 | tf_op jit(solution)/shard_map/dot_general | solution.py:61
  297.7 6.5 %all-reduce = (f32[768]{0:T(1024)S(1)}, f32[768]{0:T(1024)S(1)}) all-reduce(f32[768]{0:T(1024)S(1)} %get-tuple-element.6, f32[768]{0:T(1024)S(1)} %get-tuple-element.5), channel_id=1, replica_groups=mesh['grp'=2,'sp'=4,'tp'=4] {'tp'}, use_global_device_ids=true, to_apply=%region_9.10 | all-reduce | flops 1536 | bytes 12288 | tf_op jit(solution)/shard_map/psum | solution.py:68
  304.2 1.7 add_convert_fusion
  (46 shorter events, 11.1 us)
Async XLA Ops:
  6.5 50.8 %all-gather.9.cloned.1.call-start = ((), (), s32[]{:S(2)}) async-start(), calls=%async_computation.2 | async-start | bytes 2621440 | tf_op jit(solution)/shard_map/all_gather | solution.py:49
  8.8 53.6 %copy-start.2 = (bf16[2,256,1024]{2,1,0:T(8,128)(2,1)S(1)}, bf16[2,256,1024]{2,1,0:T(8,128)(2,1)}, u32[]{:S(2)}) copy-start(bf16[2,256,1024]{2,1,0:T(8,128)(2,1)} %param.9) | copy-start | bytes 3145732
  8.8 95.4 %all-reduce.5.cloned.1.call-start = ((), (), s32[]{:S(2)}) async-start(), calls=%async_computation | async-start | bytes 3145728 | tf_op jit(solution)/shard_map/psum | solution.py:53
  62.3 1.9 copy-start.4
  62.3 1.9 copy-start.5
  62.3 1.9 copy-start.6
  62.4 89.1 %all-gather.11.cloned.1.call-start = ((), (), s32[]{:S(2)}) async-start(), calls=%async_computation.3 | async-start | bytes 2621440 | tf_op jit(solution)/shard_map/all_gather | solution.py:63
  63.5 133.9 %all-gather.13.cloned.1.call-start = ((), (), s32[]{:S(2)}) async-start(), calls=%async_computation.4 | async-start | bytes 2621440 | tf_op jit(solution)/shard_map/all_gather | solution.py:49
  64.1 180.8 %all-reduce.7.cloned.1.call-start = ((), (), s32[]{:S(2)}) async-start(), calls=%async_computation.1 | async-start | bytes 3145728 | tf_op jit(solution)/shard_map/psum | solution.py:53
  105.3 8.8 %collective-permute-start = (bf16[1024,15]{1,0:T(8,128)(2,1)S(1)}, bf16[1024,15]{1,0:T(8,128)(2,1)S(1)}, u32[]{:S(2)}, u32[]{:S(2)}) collective-permute-start(bf16[1024,15]{1,0:T(8,128)(2,1)S(1)} %slice.138), channel_id=1, source_target_pairs={{0,4},{4,8},{8,12},{1,5},{5,9},{9,13},{2,6},{6,10},{10,14},{3,7},{... | collective-permute-start | bytes 92168 | tf_op jit(solution)/shard_map/ppermute | solution.py:17
  118.5 1.4 copy-start
  119.9 4.1 %copy-start.3 = (bf16[2,4,256,256]{3,2,1,0:T(8,128)(2,1)S(1)}, bf16[2,4,256,256]{3,2,1,0:T(8,128)(2,1)}, u32[]{:S(2)}) copy-start(bf16[2,4,256,256]{3,2,1,0:T(8,128)(2,1)} %param.10) | copy-start | bytes 3145732
  203.1 89.0 %all-gather.15.cloned.1.call-start = ((), (), s32[]{:S(2)}) async-start(), calls=%async_computation.5 | async-start | bytes 2621440 | tf_op jit(solution)/shard_map/all_gather | solution.py:63
  246.0 9.2 %collective-permute-start.1 = (bf16[1024,15]{1,0:T(8,128)(2,1)S(1)}, bf16[1024,15]{1,0:T(8,128)(2,1)S(1)}, u32[]{:S(2)}, u32[]{:S(2)}) collective-permute-start(bf16[1024,15]{1,0:T(8,128)(2,1)S(1)} %slice.149), channel_id=1, source_target_pairs={{0,4},{4,8},{8,12},{1,5},{5,9},{9,13},{2,6},{6,10},{10,14},{3,7},{... | collective-permute-start | bytes 92168 | tf_op jit(solution)/shard_map/ppermute | solution.py:17
  259.4 1.4 copy-start.1
Sparse Core Ops, SparseCore 0:
  8.9 48.3 all-gather.8
  62.5 41.6 all-reduce.4
  105.8 45.7 all-gather.10
  152.9 44.4 all-gather.12
  203.2 41.6 all-reduce.6
  246.3 45.7 all-gather.14
where the time goes:
time: 313 us
  waiting for transfers between devices  227 us (73%)
  matrix products  24.5 us (8%)
  other arithmetic  20.6 us (7%)
  between operations  13.7 us (4%)
  blocking collectives  13 us (4%)
  starting transfers between devices  7.2 us (2%)
  local copies, waits for them, and re-layouts  6.35 us (2%)
    all_gather x2, waiting for transfers between devices, per_device(): whole_in = lax.all_gather(in_weight[layer_index], 'sp', axis=0, tiled=True)  82.1 us
    psum x2, waiting for transfers between devices, per_device(): hidden = lax.psum(partial_value.astype(jnp.bfloat16), 'tp')  81.1 us
    all_gather x2, waiting for transfers between devices, per_device(): lax.all_gather(out_weight[layer_index], 'sp', axis=0, tiled=True)  52.2 us
    psum x2, blocking collectives, per_device(): lax.psum((jnp.sum(summed, axis=1), jnp.sum(summed * summed, axis=1)), 'tp')  13 us
    dot_general x2, matrix products, per_device(): lax.dot_general(scaled, lax.all_gather(out_weight[layer_index], 'sp', axi...  11.4 us
    ppermute x2, waiting for transfers between devices, passed_along(): return lax.ppermute(block, axis, route)  10.9 us
    dot_general x2, matrix products, per_device(): lax.dot_general(whole_in, current, contract_cols, preferred_element_type=...  10.6 us
    convert_element_type x2, other arithmetic, pooled_windows(): (window_sums / counts - hidden.astype(jnp.float32)).astype(jnp.bfloat16)  8.26 us
  transfers between devices with their start and end apart: 8, of which 8 were waited for; matrix products, arithmetic and copies ran while one was open for 10% of the time, Pallas kernels for 0%

commit v1 on v0

--- a/solution.py
+++ b/solution.py
@@ -50,7 +50,7 @@
         partial_value = lax.dot_general(
             whole_in, current, contract_cols, preferred_element_type=jnp.float32
         )
-        hidden = lax.psum(partial_value.astype(jnp.bfloat16), "tp")
+        hidden = jnp.sum(lax.all_gather(partial_value.astype(jnp.bfloat16), "tp"), axis=0)
         pooled = pooled_windows(hidden, tok_start)
         grouped = pooled.reshape(GROUPS, GROUP_WIDTH, tok_rows)
         mixed = jnp.einsum(

time: 313 us -> 330 us (1.054); the launches traced: 313 us -> 325 us
  other arithmetic: 20.6 us -> 33.9 us
  waiting for transfers between devices: 227 us -> 217 us
  local copies, waits for them, and re-layouts: 6.35 us -> 15.7 us
    all_gather x0 -> x2, waiting for transfers between devices: none -> 88.1 us  [per_device(): lax.all_gather(partial_value.astype(jnp.bfloat16), 'tp')]
    psum x2 -> x0, waiting for transfers between devices: 81.1 us -> none  [per_device(): hidden = lax.psum(partial_value.astype(jnp.bfloat16), 'tp')]
    all_gather x2, waiting for transfers between devices: 52.2 us -> 21.8 us  [per_device(): lax.all_gather(out_weight[layer_index], 'sp', axis=0, tiled=True)]
    reduce_sum x0 -> x2, other arithmetic: none -> 15.1 us  [per_device(): jnp.sum(lax.all_gather(partial_value.astype(jnp.bfloat16), 'tp'), axis=0)]
    all_gather x0 -> x1, local copies, waits for them, and re-layouts: none -> 11.3 us  [per_device(): lax.all_gather(partial_value.astype(jnp.bfloat16), 'tp')]
    ppermute x2, waiting for transfers between devices: 10.9 us -> 21.7 us  [passed_along(): return lax.ppermute(block, axis, route)]
  transfers between devices with their start and end apart: 8 -> 8, of which waited for: 8 -> 8; matrix products, arithmetic and copies ran while one was open for 10% -> 17% of each run, Pallas kernels for 0% -> 0%
where the time goes in v1:
time: 330 us; the launch traced here: 325 us
  waiting for transfers between devices  217 us (66%)
  other arithmetic  33.9 us (10%)
  matrix products  24.4 us (7%)
  local copies, waits for them, and re-layouts  15.7 us (5%)
  between operations  13.7 us (4%)
  blocking collectives  12.6 us (4%)
  starting transfers between devices  7.72 us (2%)
    all_gather x2, waiting for transfers between devices, per_device(): lax.all_gather(partial_value.astype(jnp.bfloat16), 'tp')  88.1 us
    all_gather x2, waiting for transfers between devices, per_device(): whole_in = lax.all_gather(in_weight[layer_index], 'sp', axis=0, tiled=True)  84.7 us
    all_gather x2, waiting for transfers between devices, per_device(): lax.all_gather(out_weight[layer_index], 'sp', axis=0, tiled=True)  21.8 us
    ppermute x2, waiting for transfers between devices, passed_along(): return lax.ppermute(block, axis, route)  21.7 us
    reduce_sum x2, other arithmetic, per_device(): jnp.sum(lax.all_gather(partial_value.astype(jnp.bfloat16), 'tp'), axis=0)  15.1 us
    psum x2, blocking collectives, per_device(): lax.psum((jnp.sum(summed, axis=1), jnp.sum(summed * summed, axis=1)), 'tp')  12.6 us
    dot_general x2, matrix products, per_device(): lax.dot_general(scaled, lax.all_gather(out_weight[layer_index], 'sp', axi...  11.4 us
    all_gather x1, local copies, waits for them, and re-layouts, per_device(): lax.all_gather(partial_value.astype(jnp.bfloat16), 'tp')  11.3 us
  transfers between devices with their start and end apart: 8, of which 8 were waited for; matrix products, arithmetic and copies ran while one was open for 17% of the time, Pallas kernels for 0%

profile of v1, /device:TPU:0, one launch (start us, length us, event | category | flops | bytes accessed | tf_op | source)
XLA Modules:
  0.0 325.4 jit_solution(9784226894225603617)
XLA Ops:
  6.5 2.3 fusion.49
  8.9 48.5 %all-gather.13.cloned.1.call-done = bf16[1,1024,1024]{2,1,0:T(8,128)(2,1)} async-done(((bf16[1,256,1024]{2,1,0:T(8,128)(2,1)}), bf16[1,1024,1024]{2,1,0:T(8,128)(2,1)}) %all-gather.13.cloned.1.call-update) | async-done | bytes 2097168 | tf_op jit(solution)/shard_map/all_gather | solution.py:49
  57.4 5.0 %fusion.22 = bf16[1024,768]{1,0:T(8,128)(2,1)} fusion(bf16[768,1024]{1,0:T(8,128)(2,1)} %param.7, bf16[1,1024,1024]{2,1,0:T(8,128)(2,1)} %all-gather.13.cloned.1.call-done), kind=kOutput, calls=%fused_computation.40 | convolution fusion | flops 1611399168 | bytes 5242880 | tf_op jit(solution)/shard_map/dot_general | solution.py:50
  64.3 43.4 %all-gather.15.cloned.1.call-done = bf16[4096,768]{1,0:T(8,128)(2,1)} async-done(((bf16[1024,768]{1,0:T(8,128)(2,1)}), bf16[4096,768]{1,0:T(8,128)(2,1)}) %all-gather.15.cloned.1.call-update) | async-done | bytes 6291472 | tf_op jit(solution)/shard_map/all_gather | solution.py:53
  107.7 4.7 %reduce_sum.60 = bf16[1024,768]{1,0:T(8,128)(2,1)S(1)} reduce(bf16[4,1024,768]{2,1,0:T(8,128)(2,1)} %bitcast.56, bf16[]{:T(256)} %constant.51.clone.1), dimensions={0}, to_apply=%region_0.0 | reduce | flops 2359296 | bytes 7864322 | tf_op jit(solution)/shard_map/reduce_sum | solution.py:53
  112.6 3.4 %collective-permute-start = (bf16[1024,15]{1,0:T(8,128)(2,1)S(1)}, bf16[1024,15]{1,0:T(8,128)(2,1)S(1)}, u32[]{:S(2)}, u32[]{:S(2)}) collective-permute-start(bf16[1024,15]{1,0:T(8,128)(2,1)S(1)} %slice.138), channel_id=1, source_target_pairs={{0,4},{4,8},{8,12},{1,5},{5,9},{9,13},{2,6},{6,10},{10,14},{3,7},{... | collective-permute-start | bytes 92168 | tf_op jit(solution)/shard_map/ppermute | solution.py:17
  116.0 11.0 %collective-permute-done = bf16[1024,15]{1,0:T(8,128)(2,1)S(1)} collective-permute-done((bf16[1024,15]{1,0:T(8,128)(2,1)S(1)}, bf16[1024,15]{1,0:T(8,128)(2,1)S(1)}, u32[]{:S(2)}, u32[]{:S(2)}) %collective-permute-start) | collective-permute-done | bytes 30752 | tf_op jit(solution)/shard_map/ppermute | solution.py:17
  130.8 4.2 %fusion.1 = bf16[1024,768]{1,0:T(8,128)(2,1)S(1)} fusion(f32[1024,782]{1,0:T(8,128)S(1)} %slice_add_fusion.5, f32[1024,780]{1,0:T(8,128)S(1)} %slice_add_fusion.4, f32[1024,776]{1,0:T(8,128)S(1)} %slice_add_fusion.3, bf16[1024,768]{1,0:T(8,128)(2,1)S(1)} %reduce_sum.60, f32[1024]{0:T(1024)S(1)} %fusion.44, f32[768]{0:T(1024)S(1)} %add_convert_fusion.2, ...), kind=kLoop, calls=%fused_computation.9 | loop fusion | flops 7864320 | bytes 15739904 | tf_op jit(solution)/shard_map/convert_element_type | solution.py:38
  135.7 20.5 %all-gather.17.cloned.1.call-done = bf16[1,1024,1024]{2,1,0:T(8,128)(2,1)} async-done(((bf16[1,256,1024]{2,1,0:T(8,128)(2,1)}), bf16[1,1024,1024]{2,1,0:T(8,128)(2,1)}) %all-gather.17.cloned.1.call-update) | async-done | bytes 2097168 | tf_op jit(solution)/shard_map/all_gather | solution.py:63
  156.2 5.8 %fusion.47 = (f32[768]{0:T(1024)S(1)}, f32[768]{0:T(1024)S(1)}, f32[768,1024]{1,0:T(8,128)}) fusion(bf16[1024,768]{1,0:T(8,128)(2,1)S(1)} %bitcast.60, bf16[1,1024,1024]{2,1,0:T(8,128)(2,1)} %all-gather.17.cloned.1.call-done, bf16[768,1024]{1,0:T(8,128)(2,1)} %param.7), kind=kOutput, calls=%fused_computation.70 | convolution fusion | flops 1615329792 | bytes 8394752 | tf_op jit(solution)/shard_map/dot_general | solution.py:61
  162.0 6.2 %all-reduce.1 = (f32[768]{0:T(1024)S(1)}, f32[768]{0:T(1024)S(1)}) all-reduce(f32[768]{0:T(1024)S(1)} %get-tuple-element.8, f32[768]{0:T(1024)S(1)} %get-tuple-element.7), channel_id=1, replica_groups=mesh['grp'=2,'sp'=4,'tp'=4] {'tp'}, use_global_device_ids=true, to_apply=%region_4.5 | all-reduce | flops 1536 | bytes 12288 | tf_op jit(solution)/shard_map/psum | solution.py:68
  168.2 36.2 %all-gather.19.cloned.1.call-done = bf16[1,1024,1024]{2,1,0:T(8,128)(2,1)} async-done(((bf16[1,256,1024]{2,1,0:T(8,128)(2,1)}), bf16[1,1024,1024]{2,1,0:T(8,128)(2,1)}) %all-gather.19.cloned.1.call-update) | async-done | bytes 2097168 | tf_op jit(solution)/shard_map/all_gather | solution.py:49
  204.4 5.5 %fusion.28 = bf16[1024,768]{0,1:T(8,128)(2,1)} fusion(bf16[1,1024,1024]{2,1,0:T(8,128)(2,1)} %all-gather.19.cloned.1.call-done, f32[768,1024]{1,0:T(8,128)} %get-tuple-element.27, f32[1024]{0:T(1024)S(1)} %bitcast.65, f32[1024]{0:T(1024)S(1)} %bitcast.63, f32[768]{0:T(1024)S(1)} %get-tuple-element.26, f32[768]{0:T(1024)S(1)} %get-tuple-element.25), kind=kOutput, calls=%fused_computation.42 | convolution fusion | flops 1615331328 | bytes 6830080 | tf_op jit(solution)/shard_map/dot_general | solution.py:50
  210.6 44.7 %all-gather.21.cloned.1.call-done = bf16[4096,768]{0,1:T(8,128)(2,1)} async-done(((bf16[1024,768]{0,1:T(8,128)(2,1)}), bf16[4096,768]{0,1:T(8,128)(2,1)}) %all-gather.21.cloned.1.call-update) | async-done | bytes 6291472 | tf_op jit(solution)/shard_map/all_gather | solution.py:53
  255.3 11.3 %reshape.69 = bf16[4,1024,768]{1,0,2:T(4,128)(2,1)} reshape(bf16[4096,768]{0,1:T(8,128)(2,1)} %all-gather.21.cloned.1.call-done) | data formatting | bytes 12582912 | tf_op jit(solution)/shard_map/all_gather | solution.py:53
  266.5 10.4 %reduce_sum.63 = bf16[1024,768]{0,1:T(8,128)(2,1)S(1)} reduce(bf16[4,1024,768]{1,0,2:T(4,128)(2,1)} %reshape.69, bf16[]{:T(256)} %constant.51.clone.1), dimensions={0}, to_apply=%region_5.6 | reduce | flops 2359296 | bytes 7864322 | tf_op jit(solution)/shard_map/reduce_sum | solution.py:53
  277.2 4.1 %collective-permute-start.1 = (bf16[1024,15]{1,0:T(8,128)(2,1)S(1)}, bf16[1024,15]{1,0:T(8,128)(2,1)}, u32[]{:S(2)}, u32[]{:S(2)}) collective-permute-start(bf16[1024,15]{1,0:T(8,128)(2,1)S(1)} %copy.15), channel_id=1, source_target_pairs={{0,4},{4,8},{8,12},{1,5},{5,9},{9,13},{2,6},{6,10},{10,14},{3,7},{... | collective-permute-start | bytes 92168 | tf_op jit(solution)/shard_map/ppermute | solution.py:17
  282.0 10.7 %collective-permute-done.1 = bf16[1024,15]{1,0:T(8,128)(2,1)} collective-permute-done((bf16[1024,15]{1,0:T(8,128)(2,1)S(1)}, bf16[1024,15]{1,0:T(8,128)(2,1)}, u32[]{:S(2)}, u32[]{:S(2)}) %collective-permute-start.1) | collective-permute-done | bytes 30752 | tf_op jit(solution)/shard_map/ppermute | solution.py:17
  292.7 1.8 maximum_convert_fusion.1
  297.5 4.2 %fusion.3 = bf16[1024,768]{1,0:T(8,128)(2,1)S(1)} fusion(f32[1024,782]{1,0:T(8,128)S(1)} %slice_add_fusion.2, f32[1024,780]{1,0:T(8,128)S(1)} %slice_add_fusion.1, f32[1024,776]{1,0:T(8,128)S(1)} %slice_add_fusion, bf16[1024,768]{1,0:T(8,128)(2,1)S(1)} %copy.16, f32[1024]{0:T(1024)S(1)} %fusion.44, f32[768]{0:T(1024)S(1)} %add_convert_fusion.2, ...), kind=kLoop, calls=%fused_computation.11 | loop fusion | flops 7864320 | bytes 15739904 | tf_op jit(solution)/shard_map/convert_element_type | solution.py:38
  301.7 1.8 multiply_convert_fusion
  304.8 5.6 %fusion.46 = (f32[768]{0:T(1024)S(1)}, f32[768]{0:T(1024)S(1)}, f32[768,1024]{1,0:T(8,128)S(1)}) fusion(bf16[1024,768]{1,0:T(8,128)(2,1)} %bitcast.59, bf16[1,1024,1024]{2,1,0:T(8,128)(2,1)} %all-gather.23.cloned.1.call-done, f32[1024]{0:T(1024)S(1)} %bitcast.66, f32[1024]{0:T(1024)S(1)} %bitcast.64, f32[768]{0:T(1024)S(1)} %get-tuple-element.26, ...), kind=kOutput, calls=%fused_computation.69 | convolution fusion | flops 1619261952 | bytes 9981952 | tf_op jit(solution)/shard_map/dot_general | solution.py:61
  310.5 6.4 %all-reduce = (f32[768]{0:T(1024)S(1)}, f32[768]{0:T(1024)S(1)}) all-reduce(f32[768]{0:T(1024)S(1)} %get-tuple-element.6, f32[768]{0:T(1024)S(1)} %get-tuple-element.5), channel_id=1, replica_groups=mesh['grp'=2,'sp'=4,'tp'=4] {'tp'}, use_global_device_ids=true, to_apply=%region_9.10 | all-reduce | flops 1536 | bytes 12288 | tf_op jit(solution)/shard_map/psum | solution.py:68
  316.9 1.7 add_convert_fusion
  (49 shorter events, 12.3 us)
Async XLA Ops:
  6.5 50.8 %all-gather.13.cloned.1.call-start = ((), (), s32[]{:S(2)}) async-start(), calls=%async_computation | async-start | bytes 2621440 | tf_op jit(solution)/shard_map/all_gather | solution.py:49
  8.8 53.6 %copy-start = (bf16[2,256,1024]{2,1,0:T(8,128)(2,1)S(1)}, bf16[2,256,1024]{2,1,0:T(8,128)(2,1)}, u32[]{:S(2)}) copy-start(bf16[2,256,1024]{2,1,0:T(8,128)(2,1)} %param.9) | copy-start | bytes 3145732
  8.8 98.9 %all-gather.15.cloned.1.call-start = ((), (), s32[]{:S(2)}) async-start(), calls=%async_computation.1 | async-start | bytes 7864320 | tf_op jit(solution)/shard_map/all_gather | solution.py:53
  62.4 1.9 copy-start.3
  62.4 1.9 copy-start.4
  62.4 1.9 copy-start.5
  62.4 93.8 %all-gather.17.cloned.1.call-start = ((), (), s32[]{:S(2)}) async-start(), calls=%async_computation.2 | async-start | bytes 2621440 | tf_op jit(solution)/shard_map/all_gather | solution.py:63
  63.5 140.9 %all-gather.19.cloned.1.call-start = ((), (), s32[]{:S(2)}) async-start(), calls=%async_computation.3 | async-start | bytes 2621440 | tf_op jit(solution)/shard_map/all_gather | solution.py:49
  64.1 191.2 %all-gather.21.cloned.1.call-start = ((), (), s32[]{:S(2)}) async-start(), calls=%async_computation.4 | async-start | bytes 7864320 | tf_op jit(solution)/shard_map/all_gather | solution.py:53
  112.6 14.5 %collective-permute-start = (bf16[1024,15]{1,0:T(8,128)(2,1)S(1)}, bf16[1024,15]{1,0:T(8,128)(2,1)S(1)}, u32[]{:S(2)}, u32[]{:S(2)}) collective-permute-start(bf16[1024,15]{1,0:T(8,128)(2,1)S(1)} %slice.138), channel_id=1, source_target_pairs={{0,4},{4,8},{8,12},{1,5},{5,9},{9,13},{2,6},{6,10},{10,14},{3,7},{... | collective-permute-start | bytes 92168 | tf_op jit(solution)/shard_map/ppermute | solution.py:17
  130.8 4.2 %copy-start.1 = (bf16[2,4,256,256]{3,2,1,0:T(8,128)(2,1)S(1)}, bf16[2,4,256,256]{3,2,1,0:T(8,128)(2,1)}, u32[]{:S(2)}) copy-start(bf16[2,4,256,256]{3,2,1,0:T(8,128)(2,1)} %param.10) | copy-start | bytes 3145732
  210.0 94.8 %all-gather.23.cloned.1.call-start = ((), (), s32[]{:S(2)}) async-start(), calls=%async_computation.5 | async-start | bytes 2621440 | tf_op jit(solution)/shard_map/all_gather | solution.py:63
  277.2 15.5 %collective-permute-start.1 = (bf16[1024,15]{1,0:T(8,128)(2,1)S(1)}, bf16[1024,15]{1,0:T(8,128)(2,1)}, u32[]{:S(2)}, u32[]{:S(2)}) collective-permute-start(bf16[1024,15]{1,0:T(8,128)(2,1)S(1)} %copy.15), channel_id=1, source_target_pairs={{0,4},{4,8},{8,12},{1,5},{5,9},{9,13},{2,6},{6,10},{10,14},{3,7},{... | collective-permute-start | bytes 92168 | tf_op jit(solution)/shard_map/ppermute | solution.py:17
  297.5 4.2 %copy-start.2 = (bf16[2,4,256,256]{3,2,1,0:T(8,128)(2,1)S(1)}, bf16[2,4,256,256]{3,2,1,0:T(8,128)(2,1)}, u32[]{:S(2)}) copy-start(bf16[2,4,256,256]{3,2,1,0:T(8,128)(2,1)} %param.10) | copy-start | bytes 3145732
Sparse Core Ops, SparseCore 0:
  8.9 48.3 all-gather.12
  62.5 45.1 all-gather.14
  109.3 46.8 all-gather.16
  157.6 46.7 all-gather.18
  210.1 45.1 all-gather.20
  256.7 48.0 all-gather.22
